TPU v7x, 32 devices: a whole 2x2x4 slice. The times are simulated.
32 devices in a mesh: ep: 16 (over z, x, core), tp: 2 (over y).
Axes of the slice: x: 2, y: 2, z: 4, core: 2. Of those that a mesh axis runs over, the one named last changes fastest.
Arguments:
- tokens: bfloat16 [2048, 2048], P('ep'), may hold values from -6 to 6
- cotangent: bfloat16 [2048, 2048], P('ep'), may hold values from -1.796875 to 1.796875
- group_weight: float32 [2048], P('ep'), may hold values from 0.2 to 1
- expert_weight: float32 [2048, 2], P('ep'), may hold values from 0.1 to 0.9
- group_choice: int32 [2048], P('ep'), may hold values from 0 to 3, as said below
- local_choice: int32 [2048, 2], P('ep'), may hold values from 0 to 3, as said below
- w_gate: bfloat16 [16, 2048, 512], P('ep', None, 'tp'), may hold values from -0.125 to 0.125
- w_up: bfloat16 [16, 2048, 512], P('ep', None, 'tp'), may hold values from -0.125 to 0.125
- w_down: bfloat16 [16, 512, 2048], P('ep', 'tp'), may hold values from -0.25 to 0.25
Outputs:
- token_grad: float32 [2048, 2048], P('ep', 'tp')
- group_weight_grad: float32 [2048], P('ep')
- expert_weight_grad: float32 [2048, 2], P('ep')
- w_gate_grad: float32 [16, 2048, 512], P('ep', None, 'tp')
- w_up_grad: float32 [16, 2048, 512], P('ep', None, 'tp')
- w_down_grad: float32 [16, 512, 2048], P('ep', 'tp')
Inputs may be any that keep to these rules, and one draw needn't show every extreme that they name: Among the 128 tokens of each device (aligned blocks of tokens), no expert 4 * group_choice + local_choice is named by more than 24 slots, and some expert is named by exactly 24 slots of every device. `local_choice`: the 2 local choices of a token differ.
All inputs are finite; a program needn't handle non-finite values.
Results may differ from a plain program's by a relative error of at most 0.006.
Values may be sent and summed in bfloat16 or wider, within the bound.
A program may use at most 64 MiB of HBM per device.

v0:
```python
import jax
import jax.numpy as jnp
from jax import lax
from jax.sharding import PartitionSpec as P

EPG = 4


def shards(
    tokens, cotangent, group_weight, expert_weight, group_choice, local_choice, w_gate, w_up, w_down
):
    token_count, feature_count = tokens.shape
    pick_count = expert_weight.shape[1]
    expert_count = lax.axis_size("ep")
    lane_count = lax.axis_size("tp")
    slot_count = token_count * pick_count
    capacity = pick_count * (3 * token_count // (2 * expert_count))
    buffer_count = expert_count * capacity
    piece_width = feature_count // lane_count
    expert_of = (group_choice[:, None] * EPG + local_choice).reshape(slot_count)
    member = (expert_of[:, None] == jnp.arange(expert_count, dtype=jnp.int32)[None, :]).astype(
        jnp.bfloat16
    )
    order = jnp.arange(slot_count, dtype=jnp.int32)
    earlier_mask = (order[:, None] > order[None, :]).astype(jnp.bfloat16)
    earlier = jnp.dot(earlier_mask, member, preferred_element_type=jnp.float32)
    position = jnp.sum(earlier * member.astype(jnp.float32), axis=1).astype(jnp.int32)
    slot_index = expert_of * capacity + position
    owner = (
        jnp.full((buffer_count,), token_count, jnp.int32).at[slot_index].set(order // pick_count)
    )
    gate_value = (group_weight[:, None] * expert_weight).astype(jnp.bfloat16).reshape(slot_count)
    gate_buffer = jnp.zeros((buffer_count,), jnp.bfloat16).at[slot_index].set(gate_value)
    start = lax.axis_index("tp") * piece_width
    token_cols = lax.dynamic_slice_in_dim(tokens, start, piece_width, 1)
    cot_cols = lax.dynamic_slice_in_dim(cotangent, start, piece_width, 1)
    token_part = jnp.take(token_cols, owner, axis=0, mode="fill", fill_value=0)
    cot_part = jnp.take(cot_cols, owner, axis=0, mode="fill", fill_value=0)
    token_part, gate_rows, cot_part = (
        lax.all_to_all(token_part, "ep", split_axis=0, concat_axis=0, tiled=True),
        lax.all_to_all(gate_buffer, "ep", split_axis=0, concat_axis=0, tiled=True),
        lax.all_to_all(cot_part, "ep", split_axis=0, concat_axis=0, tiled=True),
    )
    arrived, cot_rows = (
        lax.all_gather(token_part, "tp", axis=1, tiled=True),
        lax.all_gather(cot_part, "tp", axis=1, tiled=True),
    )
    first = w_gate[0]
    second = w_up[0]
    third = w_down[0]
    contract_cols = (((1,), (1,)), ((), ()))
    contract_rows = (((0,), (0,)), ((), ()))
    pre_gate = jnp.dot(arrived, first, preferred_element_type=jnp.float32)
    pre_up = jnp.dot(arrived, second, preferred_element_type=jnp.float32)
    back_hidden = lax.dot_general(
        cot_rows, third, contract_cols, preferred_element_type=jnp.float32
    )
    sigma = jax.nn.sigmoid(pre_gate)
    swish = pre_gate * sigma
    hidden = swish * pre_up
    gate_part = jnp.sum(hidden * back_hidden, axis=1)
    gate_float = gate_rows.reshape(buffer_count, 1).astype(jnp.float32)
    scaled = gate_float * back_hidden
    grad_gate_pre = (scaled * pre_up * sigma * (1.0 + pre_gate * (1.0 - sigma))).astype(
        jnp.bfloat16
    )
    grad_up_pre = (scaled * swish).astype(jnp.bfloat16)
    weighted = (gate_float * hidden).astype(jnp.bfloat16)
    first_grad = lax.dot_general(
        arrived, grad_gate_pre, contract_rows, preferred_element_type=jnp.float32
    )
    second_grad = lax.dot_general(
        arrived, grad_up_pre, contract_rows, preferred_element_type=jnp.float32
    )
    third_grad = lax.dot_general(
        weighted, cot_rows, contract_rows, preferred_element_type=jnp.float32
    )
    partial_value = lax.dot_general(
        grad_gate_pre, first, contract_cols, preferred_element_type=jnp.float32
    )
    partial_value = partial_value + lax.dot_general(
        grad_up_pre, second, contract_cols, preferred_element_type=jnp.float32
    )
    pieces = lax.all_to_all(partial_value, "tp", split_axis=1, concat_axis=0, tiled=True)
    row_grad = jnp.sum(pieces.reshape(lane_count, buffer_count, piece_width), axis=0).astype(
        jnp.bfloat16
    )
    gate_total = lax.psum(gate_part, "tp").astype(jnp.bfloat16)
    returned, gate_back = (
        lax.all_to_all(row_grad, "ep", split_axis=0, concat_axis=0, tiled=True),
        lax.all_to_all(gate_total, "ep", split_axis=0, concat_axis=0, tiled=True),
    )
    slot_grad = jnp.take(returned, slot_index, axis=0).astype(jnp.float32)
    token_grad = jnp.sum(slot_grad.reshape(token_count, pick_count, piece_width), axis=1)
    gate_grad = (
        jnp.take(gate_back, slot_index, axis=0).astype(jnp.float32).reshape(token_count, pick_count)
    )
    group_grad = jnp.sum(expert_weight * gate_grad, axis=1)
    expert_grad = group_weight[:, None] * gate_grad
    return (
        token_grad,
        group_grad,
        expert_grad,
        first_grad[None],
        second_grad[None],
        third_grad[None],
    )


def solution(mesh):
    in_specs = (
        P("ep", None),
        P("ep", None),
        P("ep"),
        P("ep", None),
        P("ep"),
        P("ep", None),
        P("ep", None, "tp"),
        P("ep", None, "tp"),
        P("ep", "tp", None),
    )
    out_specs = (
        P("ep", "tp"),
        P("ep"),
        P("ep", None),
        P("ep", None, "tp"),
        P("ep", None, "tp"),
        P("ep", "tp", None),
    )
    return jax.shard_map(shards, mesh=mesh, in_specs=in_specs, out_specs=out_specs, check_vma=False)
```

profile of v0, /device:TPU:9, one launch (start us, length us, event | category | flops | bytes accessed | tf_op | source)
XLA Modules:
  0.0 192.6 jit_solution(5820197067806515921)
XLA Ops:
  7.2 0.0 copy-start
  7.2 0.0 all-gather.5.cloned.1.call-start
  7.2 0.9 copy.21
  8.1 0.7 broadcast_multiply_fusion.2
  8.8 0.1 broadcast_multiply_fusion
  8.8 0.1 reshape.103
  9.0 0.2 fusion
  9.2 0.1 mul.93
  9.4 0.0 copy-start.13
  9.4 1.4 scatter_custom_fusion.1
  10.8 1.1 constant_dynamic-slice_fusion
  11.9 2.1 %gather_fusion.3 = bf16[384,1024]{1,0:T(8,128)(2,1)S(1)} fusion(bf16[128,1024]{1,0:T(8,128)(2,1)S(1)} %get-tuple-element.28, s32[1024]{0:T(1024)S(1)} %pad_clamp_fusion.1), kind=kCustom, calls=%fused_computation.1.clone | custom fusion | bytes 1574400 | tf_op jit(solution)/shard_map/jit(_take)/gather | solution.py:37
  14.0 2.1 %gather_fusion.2 = bf16[384,1024]{1,0:T(8,128)(2,1)S(1)} fusion(bf16[128,1024]{1,0:T(8,128)(2,1)S(1)} %get-tuple-element.29, s32[1024]{0:T(1024)S(1)} %pad_clamp_fusion.1), kind=kCustom, calls=%fused_computation.clone | custom fusion | bytes 1574400 | tf_op jit(solution)/shard_map/jit(_take)/gather | solution.py:38
  16.1 0.2 broadcast_select_fusion.2
  16.2 26.4 %all_to_all.69 = bf16[16,24,1024]{2,1,0:T(8,128)(2,1)} all-to-all(bf16[16,24,1024]{2,1,0:T(8,128)(2,1)S(1)} %bitcast.50), channel_id=1, replica_groups=mesh['ep'=16,'tp'=2] {'ep'}, dimensions={0} | all-to-all | bytes 1572864 | tf_op jit(solution)/shard_map/all_to_all | solution.py:40
  42.6 0.0 all-gather.5.cloned.1.call-update
  42.6 0.0 all-gather.3.cloned.1.call-start
  42.7 24.0 %all_to_all.70 = bf16[16,24,1024]{2,1,0:T(8,128)(2,1)} all-to-all(bf16[16,24,1024]{2,1,0:T(8,128)(2,1)S(1)} %bitcast.49), channel_id=1, replica_groups=mesh['ep'=16,'tp'=2] {'ep'}, dimensions={0} | all-to-all | bytes 1572864 | tf_op jit(solution)/shard_map/all_to_all | solution.py:42
  66.6 0.0 all-gather.3.cloned.1.call-update
  66.7 0.1 copy.23
  66.8 0.1 reshape.142
  67.0 2.2 %scatter_custom_fusion = bf16[384]{0:T(512)(128)(2,1)S(1)} fusion(s32[256]{0:T(256)S(1)} %bitcast.53, bf16[256]{0:T(256)(128)(2,1)S(1)} %reshape.142, bf16[]{:T(256)} %constant.47.clone.1), kind=kCustom, calls=%fused_computation.58 | custom fusion | bytes 770 | tf_op jit(solution)/shard_map/scatter | solution.py:33
  69.2 0.1 all_to_all.61
  69.3 8.7 %all_to_all.71 = bf16[16,24,1]{1,2,0:T(2,128)(2,1)S(1)} all-to-all(bf16[16,24,1]{1,2,0:T(2,128)(2,1)S(1)} %all_to_all.61), channel_id=1, replica_groups=mesh['ep'=16,'tp'=2] {'ep'}, dimensions={0} | all-to-all | bytes 1536 | tf_op jit(solution)/shard_map/all_to_all | solution.py:41
  78.0 0.1 reshape.105
  78.1 0.0 all-gather.5.cloned.1.call-done
  78.1 2.3 %fusion.3 = f32[384,256]{0,1:T(8,128)S(1)} fusion(bf16[384,2048]{1,0:T(8,128)(2,1)} %all-gather.5.cloned.1.call-done, bf16[1,2048,256]{2,1,0:T(8,128)(2,1)S(1)} %copy-done), kind=kOutput, calls=%fused_computation.15 | convolution fusion | flops 402653184 | bytes 3014656 | tf_op jit(solution)/shard_map/dot_general | solution.py:53
  80.5 0.0 copy-start.4
  80.5 2.1 %fusion.6 = f32[384,256]{0,1:T(8,128)S(1)} fusion(bf16[384,2048]{1,0:T(8,128)(2,1)S(1)} %copy-done.1, bf16[1,2048,256]{2,1,0:T(8,128)(2,1)} %param.18), kind=kOutput, calls=%fused_computation.18 | convolution fusion | flops 402653184 | bytes 3014656 | tf_op jit(solution)/shard_map/dot_general | solution.py:54
  82.6 0.0 copy-start.6
  82.6 14.8 %all-gather.3.cloned.1.call-done = bf16[384,2048]{1,0:T(8,128)(2,1)} async-done(((bf16[384,1024]{1,0:T(8,128)(2,1)}), bf16[384,2048]{1,0:T(8,128)(2,1)}) %all-gather.3.cloned.1.call-update) | async-done | bytes 1572880 | tf_op jit(solution)/shard_map/all_gather | solution.py:46
  97.4 2.5 %multiply_reduce_fusion = (f32[384]{0:T(512)S(1)}, bf16[384,256]{0,1:T(8,128)(2,1)S(1)}, bf16[384,256]{0,1:T(8,128)(2,1)S(1)}) fusion(f32[384,256]{0,1:T(8,128)S(1)} %fusion.6, f32[384,256]{0,1:T(8,128)S(1)} %fusion.3, f32[384]{0:T(512)S(1)} %reshape.105, bf16[384,2048]{1,0:T(8,128)(2,1)} %all-gather.3.cloned.1.call-done, bf16[1,256,2048]{2,1,0:T(8,128)(2,1)} %param.19), kind=kOutput, calls=%fused_computation.27 | convolution fusion | flops 404323968 | bytes 3804160 | tf_op jit(solution)/shard_map/dot_general | solution.py:55
  99.9 0.0 copy-start.8
  99.9 0.0 copy-start.2
  99.9 0.6 fusion.1
  100.6 0.0 copy-done.8
  100.6 0.1 copy-done.10
  100.7 0.6 copy-done.2
  101.3 0.6 convolution_add_fusion
  101.9 1.9 copy.31
  103.8 5.2 %all-to-all-start.3 = ((f32[384,2,1024]{2,0,1:T(8,128)}), f32[384,2,1024]{2,0,1:T(8,128)}, u32[]{:S(2)}, u32[]{:S(2)}) async-start(f32[384,2,1024]{2,0,1:T(8,128)} %bitcast.45), calls=%async_computation.3 | async-start | bytes 6291456 | tf_op jit(solution)/shard_map/all_to_all | solution.py:84
  109.0 35.5 %psum.7 = bf16[384]{0:T(512)(128)(2,1)S(1)} all-reduce(f32[384]{0:T(512)S(1)} %get-tuple-element.23), channel_id=1, replica_groups=mesh['ep'=16,'tp'=2] {'tp'}, use_global_device_ids=true, to_apply=%region_6.8 | all-reduce | flops 384 | bytes 2304 | tf_op jit(solution)/shard_map/psum | solution.py:88
  144.5 0.7 all_to_all.62
  145.3 7.3 %all-to-all-start.5 = ((bf16[16,24,1]{1,2,0:T(2,128)(2,1)}), bf16[16,24,1]{1,2,0:T(2,128)(2,1)S(1)}, u32[]{:S(2)}, u32[]{:S(2)}) async-start(bf16[16,24,1]{1,2,0:T(2,128)(2,1)} %all_to_all.62), calls=%async_computation.5 | async-start | bytes 16384 | tf_op jit(solution)/shard_map/all_to_all | solution.py:91
  152.6 3.3 %reduce_sum.46 = bf16[384,1024]{1,0:T(8,128)(2,1)} reduce(f32[384,2,1024]{2,0,1:T(8,128)} %all-to-all-done.3, f32[]{:T(128)} %constant.43.clone.1), dimensions={1}, to_apply=%region_3.5 | reduce | flops 393216 | bytes 3932164 | tf_op jit(solution)/shard_map/reduce_sum | solution.py:85
  155.8 1.4 all-to-all-done.5
  157.3 5.2 %all-to-all-start.4 = ((bf16[16,24,1024]{2,1,0:T(8,128)(2,1)}), bf16[16,24,1024]{2,1,0:T(8,128)(2,1)S(1)}, u32[]{:S(2)}, u32[]{:S(2)}) async-start(bf16[16,24,1024]{2,1,0:T(8,128)(2,1)} %bitcast.48), calls=%async_computation.4 | async-start | bytes 1572864 | tf_op jit(solution)/shard_map/all_to_all | solution.py:90
  162.5 0.8 convert_element_type.71
  163.2 0.1 copy.27
  163.3 0.7 pad_clamp_fusion
  164.0 3.0 %convolution_bitcast_fusion.1 = f32[1,2048,256]{2,1,0:T(8,128)} fusion(bf16[384,2048]{1,0:T(8,128)(2,1)S(1)} %copy-done.1, bf16[384,256]{0,1:T(8,128)(2,1)} %copy-done.10), kind=kOutput, calls=%fused_computation.9 | convolution fusion | flops 402653184 | bytes 3866624 | tf_op jit(solution)/shard_map/dot_general | solution.py:72
  167.1 2.1 %convolution_bitcast_fusion.2 = f32[1,2048,256]{2,1,0:T(8,128)} fusion(bf16[384,2048]{1,0:T(8,128)(2,1)S(1)} %copy-done.1, bf16[384,256]{0,1:T(8,128)(2,1)S(1)} %copy-done.9), kind=kOutput, calls=%fused_computation.10 | convolution fusion | flops 402653184 | bytes 3866624 | tf_op jit(solution)/shard_map/dot_general | solution.py:69
  169.2 0.0 copy-start.15
  169.2 2.1 %convolution_bitcast_fusion = f32[1,256,2048]{2,1,0:T(8,128)} fusion(bf16[384,2048]{1,0:T(8,128)(2,1)S(1)} %copy-done.3, f32[384]{0:T(512)S(1)} %reshape.105, f32[384,256]{0,1:T(8,128)S(1)} %copy-done.7, f32[384,256]{0,1:T(8,128)S(1)} %copy-done.5), kind=kOutput, calls=%fused_computation.8 | convolution fusion | flops 403341312 | bytes 4457984 | tf_op jit(solution)/shard_map/dot_general | solution.py:75
  171.3 0.1 all_to_all.60
  171.4 1.9 %gather_fusion.1 = bf16[256]{0:T(256)(128)(2,1)S(1)} fusion(bf16[384]{0:T(512)(128)(2,1)S(1)} %all_to_all.60, s32[1024]{0:T(1024)S(1)} %pad_clamp_fusion), kind=kCustom, calls=%fused_computation.3 | custom fusion | bytes 2048 | tf_op jit(solution)/shard_map/jit(_take)/gather | solution.py:96
  173.3 0.2 gather.18
  173.5 0.1 convert_multiply_fusion
  173.6 0.6 copy.28
  174.2 0.6 fusion.13
  174.9 7.3 %all-to-all-done.4 = bf16[16,24,1024]{2,1,0:T(8,128)(2,1)S(1)} async-done(((bf16[16,24,1024]{2,1,0:T(8,128)(2,1)}), bf16[16,24,1024]{2,1,0:T(8,128)(2,1)S(1)}, u32[]{:S(2)}, u32[]{:S(2)}) %all-to-all-start.4) | async-done | bytes 786464 | tf_op jit(solution)/shard_map/all_to_all | solution.py:90
  182.1 1.2 gather_fusion
  183.3 0.2 gather.16
  183.5 2.2 %convert_reduce_fusion = f32[128,1024]{1,0:T(8,128)} fusion(bf16[128,2,1024]{2,1,0:T(2,128)(2,1)S(1)} %gather.16, pred[128,2]{1,0:T(8,128)(4,1)S(1)} %get-tuple-element.20), kind=kLoop, calls=%fused_computation.22 | loop fusion | flops 655360 | bytes 1048832 | tf_op jit(solution)/shard_map/reduce_sum | solution.py:94
  (32 shorter events, 0.1 us)
Async XLA Ops:
  7.2 70.9 %copy-start = (bf16[1,2048,256]{2,1,0:T(8,128)(2,1)S(1)}, bf16[1,2048,256]{2,1,0:T(8,128)(2,1)}, u32[]{:S(2)}) copy-start(bf16[1,2048,256]{2,1,0:T(8,128)(2,1)} %param.17) | copy-start | bytes 3145732
  7.2 70.9 %all-gather.5.cloned.1.call-start = ((), (), s32[]{:S(2)}) async-start(), calls=%async_computation.7 | async-start | bytes 2359296 | tf_op jit(solution)/shard_map/all_gather | solution.py:45
  9.4 57.6 %copy-start.13 = (s32[256,1]{0,1:T(1,128)}, s32[256,1]{0,1:T(1,128)S(1)}, u32[]{:S(2)}) copy-start(s32[256,1]{0,1:T(1,128)S(1)} %compare_select_fusion.1) | copy-start | bytes 3076
  42.6 24.1 %copy-start.12 = (f32[128,2]{0,1:T(2,128)S(1)}, f32[128,2]{0,1:T(2,128)}, u32[]{:S(2)}) copy-start(f32[128,2]{0,1:T(2,128)} %param.14) | copy-start | bytes 3076
  42.6 24.1 %copy-start.14 = (f32[128]{0:T(128)S(1)}, f32[128]{0:T(128)}, u32[]{:S(2)}) copy-start(f32[128]{0:T(128)} %param.13) | copy-start | bytes 1540
  42.6 54.7 %all-gather.3.cloned.1.call-start = ((), (), s32[]{:S(2)}) async-start(), calls=%async_computation.6 | async-start | bytes 2359296 | tf_op jit(solution)/shard_map/all_gather | solution.py:46
  78.1 2.3 %copy-start.1 = (bf16[384,2048]{1,0:T(8,128)(2,1)S(1)}, bf16[384,2048]{1,0:T(8,128)(2,1)}, u32[]{:S(2)}) copy-start(bf16[384,2048]{1,0:T(8,128)(2,1)} %all-gather.5.cloned.1.call-done) | copy-start | bytes 4718596
  80.5 19.4 %copy-start.4 = (f32[384,256]{0,1:T(8,128)}, f32[384,256]{0,1:T(8,128)S(1)}, u32[]{:S(2)}) copy-start(f32[384,256]{0,1:T(8,128)S(1)} %fusion.3) | copy-start | bytes 1179652
  82.6 17.3 %copy-start.6 = (f32[384,256]{0,1:T(8,128)}, f32[384,256]{0,1:T(8,128)S(1)}, u32[]{:S(2)}) copy-start(f32[384,256]{0,1:T(8,128)S(1)} %fusion.6) | copy-start | bytes 1179652
  99.9 0.7 copy-start.8
  99.9 0.7 copy-start.10
  99.9 1.4 copy-start.2
  103.8 41.4 %all-to-all-start.3 = ((f32[384,2,1024]{2,0,1:T(8,128)}), f32[384,2,1024]{2,0,1:T(8,128)}, u32[]{:S(2)}, u32[]{:S(2)}) async-start(f32[384,2,1024]{2,0,1:T(8,128)} %bitcast.45), calls=%async_computation.3 | async-start | bytes 6291456 | tf_op jit(solution)/shard_map/all_to_all | solution.py:84
  145.3 12.0 %all-to-all-start.5 = ((bf16[16,24,1]{1,2,0:T(2,128)(2,1)}), bf16[16,24,1]{1,2,0:T(2,128)(2,1)S(1)}, u32[]{:S(2)}, u32[]{:S(2)}) async-start(bf16[16,24,1]{1,2,0:T(2,128)(2,1)} %all_to_all.62), calls=%async_computation.5 | async-start | bytes 16384 | tf_op jit(solution)/shard_map/all_to_all | solution.py:91
  157.3 24.9 %all-to-all-start.4 = ((bf16[16,24,1024]{2,1,0:T(8,128)(2,1)}), bf16[16,24,1024]{2,1,0:T(8,128)(2,1)S(1)}, u32[]{:S(2)}, u32[]{:S(2)}) async-start(bf16[16,24,1024]{2,1,0:T(8,128)(2,1)} %bitcast.48), calls=%async_computation.4 | async-start | bytes 1572864 | tf_op jit(solution)/shard_map/all_to_all | solution.py:90
  164.0 3.0 %copy-start.9 = (bf16[384,256]{0,1:T(8,128)(2,1)S(1)}, bf16[384,256]{0,1:T(8,128)(2,1)}, u32[]{:S(2)}) copy-start(bf16[384,256]{0,1:T(8,128)(2,1)} %copy-done.8) | copy-start | bytes 589828
  167.1 2.1 %copy-start.3 = (bf16[384,2048]{1,0:T(8,128)(2,1)S(1)}, bf16[384,2048]{1,0:T(8,128)(2,1)}, u32[]{:S(2)}) copy-start(bf16[384,2048]{1,0:T(8,128)(2,1)} %all-gather.3.cloned.1.call-done) | copy-start | bytes 4718596
  167.1 2.1 %copy-start.5 = (f32[384,256]{0,1:T(8,128)S(1)}, f32[384,256]{0,1:T(8,128)}, u32[]{:S(2)}) copy-start(f32[384,256]{0,1:T(8,128)} %copy-done.4) | copy-start | bytes 1179652
  167.1 2.1 %copy-start.7 = (f32[384,256]{0,1:T(8,128)S(1)}, f32[384,256]{0,1:T(8,128)}, u32[]{:S(2)}) copy-start(f32[384,256]{0,1:T(8,128)} %copy-done.6) | copy-start | bytes 1179652
  169.2 4.3 %copy-start.11 = (s32[128,2]{1,0:T(8,128)S(1)}, s32[128,2]{1,0:T(8,128)}, u32[]{:S(2)}) copy-start(s32[128,2]{1,0:T(8,128)} %convert_element_type.71) | copy-start | bytes 3076
  169.2 4.3 %copy-start.15 = (f32[128]{0:T(128)S(1)}, f32[128]{0:T(128)}, u32[]{:S(2)}) copy-start(f32[128]{0:T(128)} %param.13) | copy-start | bytes 1540
Sparse Core Ops, SparseCore 0:
  42.7 25.8 all-gather.4
  70.2 27.1 all-gather.2
where the time goes:
time: 193 us
  blocking collectives  94.5 us (49%)
  waiting for transfers between devices  23.5 us (12%)
  local copies, waits for them, and re-layouts  18.8 us (10%)
  starting transfers between devices  17.8 us (9%)
  matrix products  15.6 us (8%)
  between operations  14.4 us (7%)
  other arithmetic  7.91 us (4%)
    psum x1, blocking collectives, shards(): gate_total = lax.psum(gate_part, 'tp').astype(jnp.bfloat16)  35.5 us
    all_to_all x1, blocking collectives, shards(): lax.all_to_all(token_part, 'ep', split_axis=0, concat_axis=0, tiled=True)  26.4 us
    all_to_all x1, blocking collectives, shards(): lax.all_to_all(cot_part, 'ep', split_axis=0, concat_axis=0, tiled=True)  24 us
    all_gather x1, waiting for transfers between devices, shards(): lax.all_gather(cot_part, 'tp', axis=1, tiled=True)  14.8 us
    all_to_all x1, blocking collectives, shards(): lax.all_to_all(gate_buffer, 'ep', split_axis=0, concat_axis=0, tiled=True)  8.69 us
    all_to_all x1, starting transfers between devices, shards(): lax.all_to_all(gate_total, 'ep', split_axis=0, concat_axis=0, tiled=True)  7.32 us
    all_to_all x1, waiting for transfers between devices, shards(): lax.all_to_all(row_grad, 'ep', split_axis=0, concat_axis=0, tiled=True)  7.25 us
    all_to_all x1, starting transfers between devices, shards(): lax.all_to_all(row_grad, 'ep', split_axis=0, concat_axis=0, tiled=True)  5.21 us
  transfers between devices with their start and end apart: 5, of which 3 were waited for; matrix products, arithmetic and copies ran while one was open for 12% of the time, Pallas kernels for 0%

commit v1 on v0

--- a/solution.py
+++ b/solution.py
@@ -4,6 +4,11 @@
 from jax.sharding import PartitionSpec as P
 
 EPG = 4
+
+
+def add_all(block, axis):
+    parts = lax.all_gather(block, axis)
+    return jnp.sum(parts, axis=0)
 
 
 def shards(
@@ -85,7 +90,7 @@
     row_grad = jnp.sum(pieces.reshape(lane_count, buffer_count, piece_width), axis=0).astype(
         jnp.bfloat16
     )
-    gate_total = lax.psum(gate_part, "tp").astype(jnp.bfloat16)
+    gate_total = add_all(gate_part, "tp").astype(jnp.bfloat16)
     returned, gate_back = (
         lax.all_to_all(row_grad, "ep", split_axis=0, concat_axis=0, tiled=True),
         lax.all_to_all(gate_total, "ep", split_axis=0, concat_axis=0, tiled=True),

time: 193 us -> 193 us (level)
    psum x1 -> x0, blocking collectives: 35.5 us -> none  [shards(): gate_total = lax.psum(gate_part, 'tp').astype(jnp.bfloat16)]
    all_gather x0 -> x1, blocking collectives: none -> 35.5 us  [add_all(): parts = lax.all_gather(block, axis)]
where the time goes in v1:
time: 193 us
  blocking collectives  94.5 us (49%)
  waiting for transfers between devices  23.5 us (12%)
  local copies, waits for them, and re-layouts  18.8 us (10%)
  starting transfers between devices  17.8 us (9%)
  matrix products  15.6 us (8%)
  between operations  14.4 us (7%)
  other arithmetic  7.93 us (4%)
    all_gather x1, blocking collectives, add_all(): parts = lax.all_gather(block, axis)  35.5 us
    all_to_all x1, blocking collectives, shards(): lax.all_to_all(token_part, 'ep', split_axis=0, concat_axis=0, tiled=True)  26.4 us
    all_to_all x1, blocking collectives, shards(): lax.all_to_all(cot_part, 'ep', split_axis=0, concat_axis=0, tiled=True)  24 us
    all_gather x1, waiting for transfers between devices, shards(): lax.all_gather(cot_part, 'tp', axis=1, tiled=True)  14.8 us
    all_to_all x1, blocking collectives, shards(): lax.all_to_all(gate_buffer, 'ep', split_axis=0, concat_axis=0, tiled=True)  8.69 us
    all_to_all x1, starting transfers between devices, shards(): lax.all_to_all(gate_total, 'ep', split_axis=0, concat_axis=0, tiled=True)  7.34 us
    all_to_all x1, waiting for transfers between devices, shards(): lax.all_to_all(row_grad, 'ep', split_axis=0, concat_axis=0, tiled=True)  7.25 us
    all_to_all x1, starting transfers between devices, shards(): lax.all_to_all(row_grad, 'ep', split_axis=0, concat_axis=0, tiled=True)  5.21 us
  transfers between devices with their start and end apart: 5, of which 3 were waited for; matrix products, arithmetic and copies ran while one was open for 12% of the time, Pallas kernels for 0%

profile of v1, /device:TPU:9, one launch (start us, length us, event | category | flops | bytes accessed | tf_op | source)
XLA Modules:
  0.0 192.6 jit_solution(14050100003820684092)
XLA Ops:
  7.2 0.0 copy-start
  7.2 0.0 all-gather.7.cloned.1.call-start
  7.2 0.9 copy.21
  8.1 0.7 broadcast_multiply_fusion.2
  8.8 0.1 broadcast_multiply_fusion
  8.8 0.1 reshape.114
  9.0 0.2 fusion
  9.2 0.1 mul.93
  9.4 0.0 copy-start.13
  9.4 1.4 scatter_custom_fusion.1
  10.8 1.1 constant_dynamic-slice_fusion
  11.9 2.1 %gather_fusion.3 = bf16[384,1024]{1,0:T(8,128)(2,1)S(1)} fusion(bf16[128,1024]{1,0:T(8,128)(2,1)S(1)} %get-tuple-element.28, s32[1024]{0:T(1024)S(1)} %pad_clamp_fusion.1), kind=kCustom, calls=%fused_computation.1.clone | custom fusion | bytes 1574400 | tf_op jit(solution)/shard_map/jit(_take)/gather | solution.py:42
  14.0 2.1 %gather_fusion.2 = bf16[384,1024]{1,0:T(8,128)(2,1)S(1)} fusion(bf16[128,1024]{1,0:T(8,128)(2,1)S(1)} %get-tuple-element.29, s32[1024]{0:T(1024)S(1)} %pad_clamp_fusion.1), kind=kCustom, calls=%fused_computation.clone | custom fusion | bytes 1574400 | tf_op jit(solution)/shard_map/jit(_take)/gather | solution.py:43
  16.1 0.2 broadcast_select_fusion.2
  16.2 26.4 %all_to_all.65 = bf16[16,24,1024]{2,1,0:T(8,128)(2,1)} all-to-all(bf16[16,24,1024]{2,1,0:T(8,128)(2,1)S(1)} %bitcast.50), channel_id=1, replica_groups=mesh['ep'=16,'tp'=2] {'ep'}, dimensions={0} | all-to-all | bytes 1572864 | tf_op jit(solution)/shard_map/all_to_all | solution.py:45
  42.6 0.0 all-gather.7.cloned.1.call-update
  42.6 0.0 all-gather.5.cloned.1.call-start
  42.7 24.0 %all_to_all.66 = bf16[16,24,1024]{2,1,0:T(8,128)(2,1)} all-to-all(bf16[16,24,1024]{2,1,0:T(8,128)(2,1)S(1)} %bitcast.49), channel_id=1, replica_groups=mesh['ep'=16,'tp'=2] {'ep'}, dimensions={0} | all-to-all | bytes 1572864 | tf_op jit(solution)/shard_map/all_to_all | solution.py:47
  66.6 0.0 all-gather.5.cloned.1.call-update
  66.7 0.1 copy.23
  66.8 0.1 reshape.153
  67.0 2.2 %scatter_custom_fusion = bf16[384]{0:T(512)(128)(2,1)S(1)} fusion(s32[256]{0:T(256)S(1)} %bitcast.53, bf16[256]{0:T(256)(128)(2,1)S(1)} %reshape.153, bf16[]{:T(256)} %constant.47.clone.1), kind=kCustom, calls=%fused_computation.58 | custom fusion | bytes 770 | tf_op jit(solution)/shard_map/scatter | solution.py:38
  69.2 0.1 all_to_all.58
  69.3 8.7 %all_to_all.67 = bf16[16,24,1]{1,2,0:T(2,128)(2,1)S(1)} all-to-all(bf16[16,24,1]{1,2,0:T(2,128)(2,1)S(1)} %all_to_all.58), channel_id=1, replica_groups=mesh['ep'=16,'tp'=2] {'ep'}, dimensions={0} | all-to-all | bytes 1536 | tf_op jit(solution)/shard_map/all_to_all | solution.py:46
  78.0 0.1 reshape.116
  78.1 0.0 all-gather.7.cloned.1.call-done
  78.1 2.3 %fusion.3 = f32[384,256]{0,1:T(8,128)S(1)} fusion(bf16[384,2048]{1,0:T(8,128)(2,1)} %all-gather.7.cloned.1.call-done, bf16[1,2048,256]{2,1,0:T(8,128)(2,1)S(1)} %copy-done), kind=kOutput, calls=%fused_computation.15 | convolution fusion | flops 402653184 | bytes 3014656 | tf_op jit(solution)/shard_map/dot_general | solution.py:58
  80.5 0.0 copy-start.4
  80.5 2.1 %fusion.6 = f32[384,256]{0,1:T(8,128)S(1)} fusion(bf16[384,2048]{1,0:T(8,128)(2,1)S(1)} %copy-done.1, bf16[1,2048,256]{2,1,0:T(8,128)(2,1)} %param.18), kind=kOutput, calls=%fused_computation.18 | convolution fusion | flops 402653184 | bytes 3014656 | tf_op jit(solution)/shard_map/dot_general | solution.py:59
  82.6 0.0 copy-start.6
  82.6 14.8 %all-gather.5.cloned.1.call-done = bf16[384,2048]{1,0:T(8,128)(2,1)} async-done(((bf16[384,1024]{1,0:T(8,128)(2,1)}), bf16[384,2048]{1,0:T(8,128)(2,1)}) %all-gather.5.cloned.1.call-update) | async-done | bytes 1572880 | tf_op jit(solution)/shard_map/all_gather | solution.py:51
  97.4 2.5 %multiply_reduce_fusion = (f32[384]{0:T(512)S(1)}, bf16[384,256]{0,1:T(8,128)(2,1)S(1)}, bf16[384,256]{0,1:T(8,128)(2,1)S(1)}) fusion(f32[384,256]{0,1:T(8,128)S(1)} %fusion.6, f32[384,256]{0,1:T(8,128)S(1)} %fusion.3, f32[384]{0:T(512)S(1)} %reshape.116, bf16[384,2048]{1,0:T(8,128)(2,1)} %all-gather.5.cloned.1.call-done, bf16[1,256,2048]{2,1,0:T(8,128)(2,1)} %param.19), kind=kOutput, calls=%fused_computation.27 | convolution fusion | flops 404323968 | bytes 3804160 | tf_op jit(solution)/shard_map/dot_general | solution.py:60
  99.9 0.0 copy-start.8
  99.9 0.0 copy-start.2
  99.9 0.6 fusion.1
  100.6 0.0 copy-done.8
  100.6 0.1 copy-done.10
  100.7 0.6 copy-done.2
  101.3 0.6 convolution_add_fusion
  101.9 1.9 copy.31
  103.8 5.2 %all-to-all-start.3 = ((f32[384,2,1024]{2,0,1:T(8,128)}), f32[384,2,1024]{2,0,1:T(8,128)}, u32[]{:S(2)}, u32[]{:S(2)}) async-start(f32[384,2,1024]{2,0,1:T(8,128)} %bitcast.45), calls=%async_computation.3 | async-start | bytes 6291456 | tf_op jit(solution)/shard_map/all_to_all | solution.py:89
  109.0 35.5 %all-gather.1 = f32[2,1,384]{2,1,0:T(1,128)S(1)} all-gather(f32[1,1,384]{2,1,0:T(1,128)S(1)} %reshape.168), channel_id=2, replica_groups=mesh['ep'=16,'tp'=2] {'tp'}, dimensions={0}, use_global_device_ids=true | all-gather | bytes 4608 | tf_op jit(solution)/shard_map/all_gather | solution.py:10
  144.5 0.7 convert_element_type.96
  145.2 7.3 %all-to-all-start.5 = ((bf16[16,24,1]{1,2,0:T(2,128)(2,1)}), bf16[16,24,1]{1,2,0:T(2,128)(2,1)S(1)}, u32[]{:S(2)}, u32[]{:S(2)}) async-start(bf16[16,24,1]{1,2,0:T(2,128)(2,1)} %convert_element_type.96), calls=%async_computation.5 | async-start | bytes 16384 | tf_op jit(solution)/shard_map/all_to_all | solution.py:96
  152.6 3.3 %reduce_sum.55 = bf16[384,1024]{1,0:T(8,128)(2,1)} reduce(f32[384,2,1024]{2,0,1:T(8,128)} %all-to-all-done.3, f32[]{:T(128)} %constant.43.clone.1), dimensions={1}, to_apply=%region_3.5 | reduce | flops 393216 | bytes 3932164 | tf_op jit(solution)/shard_map/reduce_sum | solution.py:90
  155.8 1.4 all-to-all-done.5
  157.3 5.2 %all-to-all-start.4 = ((bf16[16,24,1024]{2,1,0:T(8,128)(2,1)}), bf16[16,24,1024]{2,1,0:T(8,128)(2,1)S(1)}, u32[]{:S(2)}, u32[]{:S(2)}) async-start(bf16[16,24,1024]{2,1,0:T(8,128)(2,1)} %bitcast.48), calls=%async_computation.4 | async-start | bytes 1572864 | tf_op jit(solution)/shard_map/all_to_all | solution.py:95
  162.5 0.8 convert_element_type.81
  163.2 0.1 copy.27
  163.3 0.7 pad_clamp_fusion
  164.0 3.0 %convolution_bitcast_fusion.1 = f32[1,2048,256]{2,1,0:T(8,128)} fusion(bf16[384,2048]{1,0:T(8,128)(2,1)S(1)} %copy-done.1, bf16[384,256]{0,1:T(8,128)(2,1)} %copy-done.10), kind=kOutput, calls=%fused_computation.9 | convolution fusion | flops 402653184 | bytes 3866624 | tf_op jit(solution)/shard_map/dot_general | solution.py:77
  167.1 2.1 %convolution_bitcast_fusion.2 = f32[1,2048,256]{2,1,0:T(8,128)} fusion(bf16[384,2048]{1,0:T(8,128)(2,1)S(1)} %copy-done.1, bf16[384,256]{0,1:T(8,128)(2,1)S(1)} %copy-done.9), kind=kOutput, calls=%fused_computation.10 | convolution fusion | flops 402653184 | bytes 3866624 | tf_op jit(solution)/shard_map/dot_general | solution.py:74
  169.2 0.0 copy-start.15
  169.2 2.1 %convolution_bitcast_fusion = f32[1,256,2048]{2,1,0:T(8,128)} fusion(bf16[384,2048]{1,0:T(8,128)(2,1)S(1)} %copy-done.3, f32[384]{0:T(512)S(1)} %reshape.116, f32[384,256]{0,1:T(8,128)S(1)} %copy-done.7, f32[384,256]{0,1:T(8,128)S(1)} %copy-done.5), kind=kOutput, calls=%fused_computation.8 | convolution fusion | flops 403341312 | bytes 4457984 | tf_op jit(solution)/shard_map/dot_general | solution.py:80
  171.3 0.1 all_to_all.57
  171.4 1.9 %gather_fusion.1 = bf16[256]{0:T(256)(128)(2,1)S(1)} fusion(bf16[384]{0:T(512)(128)(2,1)S(1)} %all_to_all.57, s32[1024]{0:T(1024)S(1)} %pad_clamp_fusion), kind=kCustom, calls=%fused_computation.3 | custom fusion | bytes 2048 | tf_op jit(solution)/shard_map/jit(_take)/gather | solution.py:101
  173.3 0.2 gather.18
  173.5 0.1 convert_multiply_fusion
  173.6 0.6 copy.28
  174.2 0.6 fusion.13
  174.9 7.3 %all-to-all-done.4 = bf16[16,24,1024]{2,1,0:T(8,128)(2,1)S(1)} async-done(((bf16[16,24,1024]{2,1,0:T(8,128)(2,1)}), bf16[16,24,1024]{2,1,0:T(8,128)(2,1)S(1)}, u32[]{:S(2)}, u32[]{:S(2)}) %all-to-all-start.4) | async-done | bytes 786464 | tf_op jit(solution)/shard_map/all_to_all | solution.py:95
  182.1 1.2 gather_fusion
  183.3 0.2 gather.16
  183.5 2.2 %convert_reduce_fusion = f32[128,1024]{1,0:T(8,128)} fusion(bf16[128,2,1024]{2,1,0:T(2,128)(2,1)S(1)} %gather.16, pred[128,2]{1,0:T(8,128)(4,1)S(1)} %get-tuple-element.20), kind=kLoop, calls=%fused_computation.22 | loop fusion | flops 655360 | bytes 1048832 | tf_op jit(solution)/shard_map/reduce_sum | solution.py:99
  (34 shorter events, 0.2 us)
Async XLA Ops:
  7.2 70.9 %copy-start = (bf16[1,2048,256]{2,1,0:T(8,128)(2,1)S(1)}, bf16[1,2048,256]{2,1,0:T(8,128)(2,1)}, u32[]{:S(2)}) copy-start(bf16[1,2048,256]{2,1,0:T(8,128)(2,1)} %param.17) | copy-start | bytes 3145732
  7.2 70.9 %all-gather.7.cloned.1.call-start = ((), (), s32[]{:S(2)}) async-start(), calls=%async_computation.7 | async-start | bytes 2359296 | tf_op jit(solution)/shard_map/all_gather | solution.py:50
  9.4 57.6 %copy-start.13 = (s32[256,1]{0,1:T(1,128)}, s32[256,1]{0,1:T(1,128)S(1)}, u32[]{:S(2)}) copy-start(s32[256,1]{0,1:T(1,128)S(1)} %compare_select_fusion.1) | copy-start | bytes 3076
  42.6 24.1 %copy-start.12 = (f32[128,2]{0,1:T(2,128)S(1)}, f32[128,2]{0,1:T(2,128)}, u32[]{:S(2)}) copy-start(f32[128,2]{0,1:T(2,128)} %param.14) | copy-start | bytes 3076
  42.6 24.1 %copy-start.14 = (f32[128]{0:T(128)S(1)}, f32[128]{0:T(128)}, u32[]{:S(2)}) copy-start(f32[128]{0:T(128)} %param.13) | copy-start | bytes 1540
  42.6 54.7 %all-gather.5.cloned.1.call-start = ((), (), s32[]{:S(2)}) async-start(), calls=%async_computation.6 | async-start | bytes 2359296 | tf_op jit(solution)/shard_map/all_gather | solution.py:51
  78.1 2.3 %copy-start.1 = (bf16[384,2048]{1,0:T(8,128)(2,1)S(1)}, bf16[384,2048]{1,0:T(8,128)(2,1)}, u32[]{:S(2)}) copy-start(bf16[384,2048]{1,0:T(8,128)(2,1)} %all-gather.7.cloned.1.call-done) | copy-start | bytes 4718596
  80.5 19.4 %copy-start.4 = (f32[384,256]{0,1:T(8,128)}, f32[384,256]{0,1:T(8,128)S(1)}, u32[]{:S(2)}) copy-start(f32[384,256]{0,1:T(8,128)S(1)} %fusion.3) | copy-start | bytes 1179652
  82.6 17.3 %copy-start.6 = (f32[384,256]{0,1:T(8,128)}, f32[384,256]{0,1:T(8,128)S(1)}, u32[]{:S(2)}) copy-start(f32[384,256]{0,1:T(8,128)S(1)} %fusion.6) | copy-start | bytes 1179652
  99.9 0.7 copy-start.8
  99.9 0.7 copy-start.10
  99.9 1.4 copy-start.2
  103.8 41.4 %all-to-all-start.3 = ((f32[384,2,1024]{2,0,1:T(8,128)}), f32[384,2,1024]{2,0,1:T(8,128)}, u32[]{:S(2)}, u32[]{:S(2)}) async-start(f32[384,2,1024]{2,0,1:T(8,128)} %bitcast.45), calls=%async_computation.3 | async-start | bytes 6291456 | tf_op jit(solution)/shard_map/all_to_all | solution.py:89
  145.2 12.0 %all-to-all-start.5 = ((bf16[16,24,1]{1,2,0:T(2,128)(2,1)}), bf16[16,24,1]{1,2,0:T(2,128)(2,1)S(1)}, u32[]{:S(2)}, u32[]{:S(2)}) async-start(bf16[16,24,1]{1,2,0:T(2,128)(2,1)} %convert_element_type.96), calls=%async_computation.5 | async-start | bytes 16384 | tf_op jit(solution)/shard_map/all_to_all | solution.py:96
  157.3 24.9 %all-to-all-start.4 = ((bf16[16,24,1024]{2,1,0:T(8,128)(2,1)}), bf16[16,24,1024]{2,1,0:T(8,128)(2,1)S(1)}, u32[]{:S(2)}, u32[]{:S(2)}) async-start(bf16[16,24,1024]{2,1,0:T(8,128)(2,1)} %bitcast.48), calls=%async_computation.4 | async-start | bytes 1572864 | tf_op jit(solution)/shard_map/all_to_all | solution.py:95
  164.0 3.0 %copy-start.9 = (bf16[384,256]{0,1:T(8,128)(2,1)S(1)}, bf16[384,256]{0,1:T(8,128)(2,1)}, u32[]{:S(2)}) copy-start(bf16[384,256]{0,1:T(8,128)(2,1)} %copy-done.8) | copy-start | bytes 589828
  167.1 2.1 %copy-start.3 = (bf16[384,2048]{1,0:T(8,128)(2,1)S(1)}, bf16[384,2048]{1,0:T(8,128)(2,1)}, u32[]{:S(2)}) copy-start(bf16[384,2048]{1,0:T(8,128)(2,1)} %all-gather.5.cloned.1.call-done) | copy-start | bytes 4718596
  167.1 2.1 %copy-start.5 = (f32[384,256]{0,1:T(8,128)S(1)}, f32[384,256]{0,1:T(8,128)}, u32[]{:S(2)}) copy-start(f32[384,256]{0,1:T(8,128)} %copy-done.4) | copy-start | bytes 1179652
  167.1 2.1 %copy-start.7 = (f32[384,256]{0,1:T(8,128)S(1)}, f32[384,256]{0,1:T(8,128)}, u32[]{:S(2)}) copy-start(f32[384,256]{0,1:T(8,128)} %copy-done.6) | copy-start | bytes 1179652
  169.2 4.3 %copy-start.11 = (s32[128,2]{1,0:T(8,128)S(1)}, s32[128,2]{1,0:T(8,128)}, u32[]{:S(2)}) copy-start(s32[128,2]{1,0:T(8,128)} %convert_element_type.81) | copy-start | bytes 3076
  169.2 4.3 %copy-start.15 = (f32[128]{0:T(128)S(1)}, f32[128]{0:T(128)}, u32[]{:S(2)}) copy-start(f32[128]{0:T(128)} %param.13) | copy-start | bytes 1540
Sparse Core Ops, SparseCore 0:
  42.7 25.8 all-gather.6
  70.2 27.1 all-gather.4
